TPU v7x, 256 devices: a whole 4x4x8 slice. The times are simulated.
256 devices in a mesh: sp: 64 (over z, y, core), tp: 4 (over x).
Axes of the slice: x: 4, y: 4, z: 8, core: 2. Of those that a mesh axis runs over, the one named last changes fastest.
Arguments:
- queries: bfloat16 [8192, 2048], P('sp', 'tp'), may hold values from -6 to 6
- keys: bfloat16 [8192, 512], P('sp', 'tp'), may hold values from -6 to 6
- values: bfloat16 [8192, 512], P('sp', 'tp'), may hold values from -6 to 6
- query_gain: float32 [128], replicated, may hold values from 0.3 to 7
- key_norm_gain: float32 [128], replicated, may hold values from 0.3 to 7
- out_weight: bfloat16 [2048, 2048], P('tp'), may hold values from -0.25 to 0.25
- residual: bfloat16 [8192, 2048], P(('sp', 'tp')), may hold values from -6 to 6
- norm_gain: float32 [2048], replicated, may hold values from 0.1 to 1.9
- expert_gate: bfloat16 [64, 2048, 3072], P('sp', None, 'tp'), may hold values from -0.125 to 0.125
- expert_up: bfloat16 [64, 2048, 3072], P('sp', None, 'tp'), may hold values from -0.125 to 0.125
- expert_down: bfloat16 [64, 3072, 2048], P('sp', 'tp'), may hold values from -0.109375 to 0.109375
- routes: int32 [8192, 2], P(('sp', 'tp')), may hold values from 0 to 63, all different within a row; in each aligned block of 32 rows (0 to 31, 32 to 63, ...) at most 2 rows name the same one
- route_weight: float32 [8192, 2], P(('sp', 'tp')), may hold values from 0.25 to 1
Outputs:
- mixed: bfloat16 [8192, 2048], P(('sp', 'tp'))
Inputs may be any that keep to these rules, and one draw needn't show every extreme that they name: The two experts of a token differ. In each aligned block of 32 tokens (the tokens of one device), no expert is named by more than 2 routes, and in some block one expert is named by exactly 2.
All inputs are finite; a program needn't handle non-finite values.
Results may differ from a plain program's by a relative error of at most 0.013.
The roundings to bfloat16 on the way count: a program that leaves them out, or rounds other values in their place, can miss the bound.
Values may be sent and summed in bfloat16 or wider, within the bound.
A program may use at most 64 MiB of HBM per device.

v0:
```python
import math

import jax
import jax.numpy as jnp
from jax import lax
from jax.sharding import PartitionSpec as P

HEAD_SIZE = 128
GRID_W = 64


norm_eps = 1e-06
theta_base = 10000.0


def in_one_piece(arrays, axis, dim, along):
    both = jnp.concatenate(arrays, axis=along)
    result, at, finished = (lax.all_gather(both, axis, axis=dim, tiled=True), 0, [])
    for a in arrays:
        finished.append(lax.slice_in_dim(result, at, at + a.shape[along], axis=along))
        at += a.shape[along]
    return tuple(finished)


def in_blocks(value, dim, size):
    before, after = (value.shape[:dim], value.shape[dim + 1 :])
    return jnp.moveaxis(value.reshape(*before, size, -1, *after), dim, 0)


def sent_and_summed(value, axis, dim):
    pieces = in_blocks(value, dim, lax.axis_size(axis))
    arrived = lax.all_to_all(pieces, axis, split_axis=0, concat_axis=0, tiled=True)
    return arrived.astype(jnp.float32).sum(axis=0)


def joined_along(pieces, dim):
    dims = list(pieces.shape[1:])
    dims[dim] *= pieces.shape[0]
    return jnp.moveaxis(pieces, 0, dim).reshape(dims)


def copy_for_each(value, axis):
    size = lax.axis_size(axis)
    return lax.all_to_all(
        jnp.broadcast_to(value[None], (size, *value.shape)), axis, 0, 0, tiled=True
    )


def collect(value, axis, dim):
    return joined_along(copy_for_each(value, axis), dim)


def head_normalize(packed, gain, heads):
    heads_float = packed.astype(jnp.float32).reshape(packed.shape[0], heads, HEAD_SIZE)
    scaled = heads_float * lax.rsqrt(
        jnp.mean(heads_float * heads_float, axis=-1, keepdims=True) + norm_eps
    )
    return scaled * gain


def rotary_tables(positions):
    freq_count = HEAD_SIZE // 4
    grid_row = (positions // GRID_W).astype(jnp.float32)
    grid_col = (positions % GRID_W).astype(jnp.float32)
    inverse = theta_base ** (-jnp.arange(freq_count, dtype=jnp.float32) * 2.0 / (HEAD_SIZE // 2))
    by_row = grid_row[:, None] * inverse
    by_col = grid_col[:, None] * inverse
    angles = jnp.concatenate([by_row, by_row, by_col, by_col], axis=-1)
    return (jnp.cos(angles), jnp.sin(angles))


def apply_rotation(heads_float, cosine_table, sine_values):
    freq_count = HEAD_SIZE // 4
    split_head = heads_float.reshape(heads_float.shape[:-1] + (2, 2, freq_count))
    turned = jnp.stack([-split_head[..., 1, :], split_head[..., 0, :]], axis=-2).reshape(
        heads_float.shape
    )
    return heads_float * cosine_table[:, None, :] + turned * sine_values[:, None, :]


def on_device(
    queries,
    keys,
    values,
    query_gain,
    key_norm_gain,
    out_weight,
    residual,
    norm_gain,
    expert_gate,
    expert_up,
    expert_down,
    routes,
    route_weight,
):
    local_rows = queries.shape[0]
    query_heads = queries.shape[1] // HEAD_SIZE
    key_heads = keys.shape[1] // HEAD_SIZE
    group_members = query_heads // key_heads
    score_scale = 1.0 / math.sqrt(HEAD_SIZE)
    positions = lax.axis_index("sp") * local_rows + jnp.arange(local_rows, dtype=jnp.int32)
    cosine_table, sine_values = rotary_tables(positions)
    rotated_queries = apply_rotation(
        head_normalize(queries, query_gain, query_heads), cosine_table, sine_values
    ).astype(jnp.bfloat16)
    query_block = rotated_queries.reshape(
        local_rows, key_heads, group_members, HEAD_SIZE
    ).transpose(1, 2, 0, 3)
    query_block = query_block.reshape(key_heads, group_members * local_rows, HEAD_SIZE)
    rotated_keys = apply_rotation(
        head_normalize(keys, key_norm_gain, key_heads), cosine_table, sine_values
    ).astype(jnp.bfloat16)
    rotated_keys = rotated_keys.reshape(local_rows, key_heads * HEAD_SIZE)
    start_state = (
        jnp.full((key_heads, group_members * local_rows), -1e30, jnp.float32),
        jnp.zeros((key_heads, group_members * local_rows), jnp.float32),
        jnp.zeros((key_heads, group_members * local_rows, HEAD_SIZE), jnp.float32),
    )
    folded = start_state
    key_piece, value_piece = in_one_piece((rotated_keys, values), "sp", 0, 1)
    key_count = key_piece.shape[0]
    span_size = 512
    key_spans = key_piece.reshape(key_count // span_size, span_size, key_heads, HEAD_SIZE)
    value_spans = value_piece.reshape(key_count // span_size, span_size, key_heads, HEAD_SIZE)

    def one_span(state, span_pair):
        running, norm_sum, gathered_sum = state
        key_span, value_span = span_pair
        scores = (
            jnp.einsum("hqd,khd->hqk", query_block, key_span, preferred_element_type=jnp.float32)
            * score_scale
        )
        newest = jnp.maximum(running, jnp.max(scores, axis=-1))
        shrink = jnp.exp(running - newest)
        weights = jnp.exp(scores - newest[..., None])
        norm_sum = norm_sum * shrink + jnp.sum(weights, axis=-1)
        gathered_sum = gathered_sum * shrink[..., None] + jnp.einsum(
            "hqk,khd->hqd",
            weights.astype(jnp.bfloat16),
            value_span,
            preferred_element_type=jnp.float32,
        )
        return ((newest, norm_sum, gathered_sum), None)

    folded, _ = lax.scan(one_span, folded, (key_spans, value_spans))
    running, norm_sum, gathered_sum = folded
    attention = (gathered_sum / norm_sum[..., None]).reshape(
        key_heads, group_members, local_rows, HEAD_SIZE
    )
    attention = (
        attention.transpose(2, 0, 1, 3)
        .reshape(local_rows, query_heads * HEAD_SIZE)
        .astype(jnp.bfloat16)
    )
    out_rows = residual.shape[0]
    model_width = residual.shape[1]
    projected = sent_and_summed(
        jnp.dot(attention, out_weight, preferred_element_type=jnp.float32).astype(jnp.bfloat16),
        "tp",
        0,
    )
    hidden_state = residual.astype(jnp.float32) + projected
    normed = (
        hidden_state
        * lax.rsqrt(jnp.mean(hidden_state * hidden_state, axis=-1, keepdims=True) + norm_eps)
        * norm_gain
    ).astype(jnp.bfloat16)
    route_top = routes.shape[1]
    group_width = lax.axis_size("tp")
    expert_count = lax.axis_size("sp") * expert_gate.shape[0]
    capacity = 2 * max(1, route_top * local_rows // (group_width * expert_count))
    flat_routes = routes.reshape(-1)
    onehot = (flat_routes[:, None] == jnp.arange(expert_count, dtype=jnp.int32)[None, :]).astype(
        jnp.int32
    )
    earlier = jnp.cumsum(onehot, axis=0) - onehot
    slot_rank = jnp.sum(earlier * onehot, axis=1)
    slot_index = flat_routes * capacity + slot_rank
    placer = (
        jnp.arange(expert_count * capacity, dtype=jnp.int32)[:, None] == slot_index[None, :]
    ).astype(jnp.bfloat16)
    route_rows = jnp.repeat(normed, route_top, axis=0)
    buffer = jnp.dot(placer, route_rows, preferred_element_type=jnp.float32).astype(jnp.bfloat16)
    buffer = buffer.reshape(expert_count, capacity, model_width)
    mail_rows = lax.all_to_all(buffer, "sp", split_axis=0, concat_axis=0, tiled=True)
    inbox_rows = collect(mail_rows, "tp", 1)
    source_count = inbox_rows.shape[0]
    rows_in = inbox_rows.reshape(-1, model_width)
    gate_proj = jnp.dot(rows_in, expert_gate[0], preferred_element_type=jnp.float32)
    up_proj = jnp.dot(rows_in, expert_up[0], preferred_element_type=jnp.float32)
    hidden_act = (jax.nn.silu(gate_proj) * up_proj).astype(jnp.bfloat16)
    down_part = jnp.dot(hidden_act, expert_down[0], preferred_element_type=jnp.float32)
    down_part = down_part.reshape(source_count, group_width * capacity, model_width)
    summed = lax.psum_scatter(down_part.astype(jnp.bfloat16), "tp", scatter_dimension=1, tiled=True)
    returned = lax.all_to_all(summed, "sp", split_axis=0, concat_axis=0, tiled=True)
    per_route = jnp.dot(
        placer.T, returned.reshape(-1, model_width), preferred_element_type=jnp.float32
    )
    per_route = per_route.reshape(out_rows, route_top, model_width)
    moe_sum = jnp.sum(route_weight[:, :, None] * per_route, axis=1)
    return (hidden_state + moe_sum).astype(jnp.bfloat16)


def solution(mesh):
    placed = (
        P("sp", "tp"),
        P("sp", "tp"),
        P("sp", "tp"),
        P(),
        P(),
        P("tp", None),
        P(("sp", "tp"), None),
        P(),
        P("sp", None, "tp"),
        P("sp", None, "tp"),
        P("sp", "tp", None),
        P(("sp", "tp"), None),
        P(("sp", "tp"), None),
    )
    return jax.shard_map(
        on_device, mesh=mesh, in_specs=placed, out_specs=P(("sp", "tp"), None), check_vma=False
    )
```

profile of v0, /device:TPU:1, one launch (start us, length us, event | category | flops | bytes accessed | tf_op | source)
XLA Modules:
  0.0 365.2 jit_solution(8296184017949517132)
XLA Ops:
  20.1 71.9 %all-gather.2.cloned.1.call-done = bf16[8192,256]{0,1:T(8,128)(2,1)} async-done(((bf16[128,256]{0,1:T(8,128)(2,1)}), bf16[8192,256]{0,1:T(8,128)(2,1)}) %all-gather.2.cloned.1.call-update) | async-done | bytes 4194320 | tf_op jit(solution)/shard_map/all_gather | solution.py:18
  92.0 4.6 %fusion.46 = (bf16[8192,128]{0,1:T(8,128)(2,1)}, bf16[8192,128]{0,1:T(8,128)(2,1)}) fusion(bf16[8192,256]{0,1:T(8,128)(2,1)} %all-gather.2.cloned.1.call-done), kind=kLoop, calls=%fused_computation.84 | loop fusion | bytes 8388608 | tf_op jit(solution)/shard_map/slice | solution.py:20
  96.6 4.1 %copy.57 = bf16[8192,128]{1,0:T(8,128)(2,1)} copy(bf16[8192,128]{0,1:T(8,128)(2,1)} %get-tuple-element.115) | data formatting | bytes 4194304 | tf_op jit(solution)/shard_map/slice | solution.py:20
  100.7 4.1 %copy.54 = bf16[8192,128]{1,0:T(8,128)(2,1)} copy(bf16[8192,128]{0,1:T(8,128)(2,1)} %get-tuple-element.116) | data formatting | bytes 4194304 | tf_op jit(solution)/shard_map/slice | solution.py:20
  104.8 84.0 %while.15 = (s32[]{:T(128)}, f32[1,512]{1,0:T(1,128)S(1)}, f32[1,512]{1,0:T(1,128)S(1)}, f32[1,512,128]{2,1,0:T(8,128)S(1)}, bf16[16,512,1,128]{3,1,2,0:T(8,128)...) while((s32[]{:T(128)}, f32[1,512]{1,0:T(1,128)S(1)}, ...), condition=%wide.region_5.6_spmd.clone, body=%wide.region_2.5_spmd.clone.sunk | while | flops 135989760 | bytes 4097129 | solution.py:145
  115.3 2.2 fusion.62
  136.3 2.2 fusion.62
  157.3 2.2 fusion.62
  178.3 2.2 fusion.62
  189.1 2.9 convolution_convert_fusion.1
  192.0 4.1 %all-to-all-start = ((bf16[4,32,2048]{2,1,0:T(8,128)(2,1)}), bf16[4,32,2048]{2,1,0:T(8,128)(2,1)}, u32[]{:S(2)}, u32[]{:S(2)}) async-start(bf16[4,32,2048]{2,1,0:T(8,128)(2,1)} %bitcast.99), calls=%async_computation | async-start | bytes 1048576 | tf_op jit(solution)/shard_map/all_to_all | solution.py:32
  196.5 8.8 %all-to-all-done = bf16[4,32,2048]{2,1,0:T(8,128)(2,1)} async-done(((bf16[4,32,2048]{2,1,0:T(8,128)(2,1)}), bf16[4,32,2048]{2,1,0:T(8,128)(2,1)}, u32[]{:S(2)}, u32[]{:S(2)}) %all-to-all-start) | async-done | bytes 524320 | tf_op jit(solution)/shard_map/all_to_all | solution.py:32
  211.4 2.2 reshape.346
  213.6 27.0 %all_to_all.20 = bf16[64,2,2048]{2,1,0:T(2,128)(2,1)S(1)} all-to-all(bf16[64,2,2048]{2,1,0:T(2,128)(2,1)} %reshape.346), channel_id=1, replica_groups=mesh['sp'=64,'tp'=4] {'sp'}, dimensions={0} | all-to-all | bytes 1048576 | tf_op jit(solution)/shard_map/all_to_all | solution.py:185
  241.9 28.5 %all_to_all.21 = bf16[4,64,2,2048]{3,2,1,0:T(2,128)(2,1)S(1)} all-to-all(bf16[4,64,2,2048]{3,2,1,0:T(2,128)(2,1)S(1)} %broadcast_in_dim.14), channel_id=1, replica_groups=mesh['sp'=64,'tp'=4] {'tp'}, dimensions={0} | all-to-all | bytes 4194304 | tf_op jit(solution)/shard_map/all_to_all | solution.py:44
  270.4 3.8 %copy.62 = bf16[64,4,2,2048]{3,2,1,0:T(2,128)(2,1)} copy(bf16[64,4,2,2048]{3,2,0,1:T(2,128)(2,1)S(1)} %bitcast.93) | data formatting | bytes 4194304 | tf_op jit(solution)/shard_map/transpose | solution.py:39
  274.2 4.1 %reshape_reshape.3 = bf16[512,2048]{1,0:T(8,128)(2,1)} reshape(bf16[64,4,2,2048]{3,2,1,0:T(2,128)(2,1)} %copy.62) | data formatting | bytes 4194304 | tf_op jit(solution)/shard_map/reshape;reshape | solution.py:188
  278.3 5.5 %fusion.19 = f32[512,768]{1,0:T(8,128)} fusion(bf16[512,2048]{1,0:T(8,128)(2,1)} %reshape_reshape.3, bf16[1,2048,768]{2,1,0:T(8,128)(2,1)} %param.23), kind=kOutput, calls=%fused_computation.25 | convolution fusion | flops 1610612736 | bytes 6815744 | tf_op jit(solution)/shard_map/dot_general | solution.py:189
  283.8 8.2 %fusion.21 = bf16[64,8,2048]{2,1,0:T(8,128)(2,1)} fusion(bf16[1,768,2048]{2,1,0:T(8,128)(2,1)S(1)} %copy-done, bf16[512,2048]{1,0:T(8,128)(2,1)} %reshape_reshape.3, bf16[1,2048,768]{2,1,0:T(8,128)(2,1)} %param.24, f32[512,768]{1,0:T(8,128)} %fusion.19), kind=kOutput, calls=%fused_computation.27 | convolution fusion | flops 3224633344 | bytes 12058624 | tf_op jit(solution)/shard_map/dot_general | solution.py:192
  292.0 4.1 %copy.63 = bf16[64,8,2048]{2,0,1:T(8,128)(2,1)} copy(bf16[64,8,2048]{2,1,0:T(8,128)(2,1)} %fusion.21) | data formatting | bytes 4194304 | tf_op jit(solution)/shard_map/convert_element_type | solution.py:194
  296.1 27.3 %reduce-scatter.2.cloned.1.call-done = bf16[64,2,2048]{2,0,1:T(8,128)(2,1)} async-done(((bf16[64,8,2048]{2,0,1:T(8,128)(2,1)}), bf16[64,2,2048]{2,0,1:T(8,128)(2,1)}) %reduce-scatter.2.cloned.1.call-update) | async-done | bytes 524304 | tf_op jit(solution)/shard_map/reduce_scatter | solution.py:194
  323.4 2.4 copy.64
  325.8 10.9 %all-to-all-start.3 = ((bf16[64,2,2048]{2,1,0:T(2,128)(2,1)}), bf16[64,2,2048]{2,1,0:T(2,128)(2,1)}, u32[]{:S(2)}, u32[]{:S(2)}) async-start(bf16[64,2,2048]{2,1,0:T(2,128)(2,1)} %copy.64), calls=%async_computation.4 | async-start | bytes 1048576 | tf_op jit(solution)/shard_map/all_to_all | solution.py:195
  338.1 16.2 %all-to-all-done.3 = bf16[64,2,2048]{2,1,0:T(2,128)(2,1)} async-done(((bf16[64,2,2048]{2,1,0:T(2,128)(2,1)}), bf16[64,2,2048]{2,1,0:T(2,128)(2,1)}, u32[]{:S(2)}, u32[]{:S(2)}) %all-to-all-start.3) | async-done | bytes 524320 | tf_op jit(solution)/shard_map/all_to_all | solution.py:195
  (150 shorter events, 101.6 us)
Async XLA Ops:
  6.5 277.2 %copy-start = (bf16[1,768,2048]{2,1,0:T(8,128)(2,1)S(1)}, bf16[1,768,2048]{2,1,0:T(8,128)(2,1)}, u32[]{:S(2)}) copy-start(bf16[1,768,2048]{2,1,0:T(8,128)(2,1)} %param.25) | copy-start | bytes 9437188
  6.5 8.6 %copy-start.3 = (f32[128]{0:T(128)S(1)}, f32[128]{0:T(128)}, u32[]{:S(2)}) copy-start(f32[128]{0:T(128)} %param.18) | copy-start | bytes 1540
  6.5 85.4 %all-gather.2.cloned.1.call-start = ((), (), s32[]{:S(2)}) async-start(), calls=%async_computation.5 | async-start | bytes 4259840 | tf_op jit(solution)/shard_map/all_gather | solution.py:18
  189.1 17.4 %copy-start.1 = (bf16[32,2048]{1,0:T(8,128)(2,1)S(1)}, bf16[32,2048]{1,0:T(8,128)(2,1)}, u32[]{:S(2)}) copy-start(bf16[32,2048]{1,0:T(8,128)(2,1)} %param.21) | copy-start | bytes 393220
  189.1 17.6 %copy-start.2 = (f32[2048]{0:T(1024)S(1)}, f32[2048]{0:T(1024)}, u32[]{:S(2)}) copy-start(f32[2048]{0:T(1024)} %param.22) | copy-start | bytes 24580
  192.0 13.4 %all-to-all-start = ((bf16[4,32,2048]{2,1,0:T(8,128)(2,1)}), bf16[4,32,2048]{2,1,0:T(8,128)(2,1)}, u32[]{:S(2)}, u32[]{:S(2)}) async-start(bf16[4,32,2048]{2,1,0:T(8,128)(2,1)} %bitcast.99), calls=%async_computation | async-start | bytes 1048576 | tf_op jit(solution)/shard_map/all_to_all | solution.py:32
  196.1 127.2 %reduce-scatter.2.cloned.1.call-start = ((), (), s32[]{:S(2)}) async-start(), calls=%async_computation.6 | async-start | bytes 2621440 | tf_op jit(solution)/shard_map/reduce_scatter | solution.py:194
  325.8 28.5 %all-to-all-start.3 = ((bf16[64,2,2048]{2,1,0:T(2,128)(2,1)}), bf16[64,2,2048]{2,1,0:T(2,128)(2,1)}, u32[]{:S(2)}, u32[]{:S(2)}) async-start(bf16[64,2,2048]{2,1,0:T(2,128)(2,1)} %copy.64), calls=%async_computation.4 | async-start | bytes 1048576 | tf_op jit(solution)/shard_map/all_to_all | solution.py:195
Sparse Core Ops, SparseCore 0:
  11.6 80.3 all-gather.1
  296.2 27.1 reduce-scatter.1
where the time goes:
time: 368 us; the launch traced here: 365 us
  waiting for transfers between devices  124 us (34%)
  matrix products  80.3 us (22%)
  blocking collectives  55.5 us (15%)
  local copies, waits for them, and re-layouts  43.1 us (12%)
  other arithmetic  32.9 us (9%)
  starting transfers between devices  15.1 us (4%)
  between operations  13.6 us (4%)
    all_gather x1, waiting for transfers between devices, in_one_piece(): lax.all_gather(both, axis, axis=dim, tiled=True)  71.9 us
    dot_general x16, matrix products, one_span(): jnp.einsum('hqd,khd->hqk', query_block, key_span, preferred_element_type=...  34.9 us
    all_to_all x1, blocking collectives, copy_for_each(): lax.all_to_all(jnp.broadcast_to(value[None], (size, *value.shape)), axis,...  28.5 us
    reduce_scatter x1, waiting for transfers between devices, on_device(): lax.psum_scatter(down_part.astype(jnp.bfloat16), 'tp', scatter_dimension=...  27.3 us
    all_to_all x1, blocking collectives, on_device(): lax.all_to_all(buffer, 'sp', split_axis=0, concat_axis=0, tiled=True)  27 us
    dot_general x16, matrix products, one_span(): jnp.einsum('hqk,khd->hqd', weights.astype(jnp.bfloat16), value_span, pref...  25.5 us
    reduce_sum x16, other arithmetic, one_span(): norm_sum = norm_sum * shrink + jnp.sum(weights, axis=-1)  22.6 us
    all_to_all x1, waiting for transfers between devices, on_device(): lax.all_to_all(summed, 'sp', split_axis=0, concat_axis=0, tiled=True)  16.2 us
  transfers between devices with their start and end apart: 4, of which 4 were waited for; matrix products, arithmetic and copies ran while one was open for 3% of the time, Pallas kernels for 0%

commit v1 on v0

v1 whole, which is shorter than its diff:
```python
import functools
import math

import jax
import jax.numpy as jnp
import numpy as np
from jax import lax
from jax.experimental import pallas as pl
from jax.experimental.pallas import tpu as pltpu
from jax.sharding import PartitionSpec as P

HEAD_SIZE = 128
GRID_W = 64
NZ, NY = 8, 4
MESH = pl.DeviceIdType.MESH

norm_eps = 1e-06
theta_base = 10000.0


def _signed(count):
    half = count // 2
    return [0] + [s * m for m in range(1, half) for s in (1, -1)] + [half]


ORDER = sorted(
    [(dz, dy) for dz in _signed(NZ) for dy in _signed(NY)],
    key=lambda d: (abs(d[0]) + abs(d[1]), min(abs(d[0]), abs(d[1]))),
)


def _onward(d, count):
    half = count // 2
    if d == 0:
        return [(1, 0), (1, 1), (-1, 0), (-1, 1)]
    if d == half:
        return []
    if d > 0:
        return [(1, 0)] if d == half - 1 else [(1, 0), (1, 1)]
    return [(-1, 1)] if d == 1 - half else [(-1, 0), (-1, 1)]


def forwards(core, dz, dy):
    both = [(1, 0), (1, 1), (-1, 0), (-1, 1)]
    out = []
    if core == 0:
        if dy == 0:
            out += [("z", s, p) for s, p in _onward(dz, NZ)]
            out += [("y", s, p) for s, p in both]
        else:
            out += [("y", s, p) for s, p in _onward(dy, NY)]
    else:
        if dz == 0:
            out += [("y", s, p) for s, p in _onward(dy, NY)]
            out += [("z", s, p) for s, p in both]
        else:
            out += [("z", s, p) for s, p in _onward(dz, NZ)]
    return out


def attend_kernel(
    q_in, k_in, v_in, qg, kg, rowtab, colcos, colsin, outw_hbm, resid, ng,
    state_out, normed_out,
    kv, q_scr, m_scr, l_scr, acc, outw, part_out, part_in,
    send_sem, recv_sem, w_sem, xs_sem, xr_sem,
):
    me = lax.axis_index("sp")
    t = lax.axis_index("tp")
    z, y, c = me // 8, (me // 2) % NY, me % 2
    chip = me // 2

    wcopy = pltpu.make_async_copy(outw_hbm, outw, w_sem)
    wcopy.start()

    def sp_of(zz, yy, cc):
        return (zz % NZ) * 8 + (yy % NY) * 2 + cc

    near = {
        ("z", 1): sp_of(z + 1, y, c),
        ("z", -1): sp_of(z + NZ - 1, y, c),
        ("y", 1): sp_of(z, y + 1, c),
        ("y", -1): sp_of(z, y + NY - 1, c),
    }
    mate = sp_of(z, y, 1 - c)

    barrier = pltpu.get_barrier_semaphore()
    for peer in list(near.values()) + [mate]:
        pl.semaphore_signal(barrier, inc=1, device_id=(peer, t), device_id_type=MESH)
    for k in range(1, 4):
        pl.semaphore_signal(barrier, inc=1, device_id=(me, (t + k) % 4), device_id_type=MESH)

    lane = lax.broadcasted_iota(jnp.int32, (64, 128), 1)
    low = lane < 64

    def table(row, col):
        return jnp.concatenate(
            [
                jnp.where(low, jnp.broadcast_to(rowtab[row : row + 1, :], (64, 128)), col),
                jnp.where(low, jnp.broadcast_to(rowtab[row + 1 : row + 2, :], (64, 128)), col),
            ],
            axis=0,
        )

    cos = table(0, colcos[...])
    sin = table(2, colsin[...])
    even = ((lax.broadcasted_iota(jnp.int32, (128, 128), 1) // 32) % 2) == 0
    sin_a = jnp.where(even, -sin, 0.0)
    sin_b = jnp.where(even, 0.0, sin)

    def turn(x, gain):
        x = x.astype(jnp.float32)
        x = x * lax.rsqrt(jnp.mean(x * x, axis=-1, keepdims=True) + norm_eps) * gain
        return x * cos + pltpu.roll(x, 96, 1) * sin_a + pltpu.roll(x, 32, 1) * sin_b

    key = turn(k_in[...], kg[...]).astype(jnp.bfloat16).astype(jnp.float32)
    kv[chip, c, 0] = jnp.transpose(key).astype(jnp.bfloat16)
    kv[chip, c, 1] = v_in[...]
    pl.semaphore_wait(barrier, 8)

    def remote(slot, core, part, peer, group):
        return pltpu.make_async_remote_copy(
            src_ref=kv.at[slot, core, part],
            dst_ref=kv.at[slot, core, part],
            send_sem=send_sem.at[group],
            recv_sem=recv_sem.at[slot, core, part],
            device_id=(peer, t),
            device_id_type=MESH,
        )

    def slot_at(dz, dy):
        return ((z + NZ - dz) % NZ) * NY + (y + NY - dy) % NY

    def take(dz, dy):
        slot = slot_at(dz, dy)
        for part in range(2):
            if (dz, dy) != (0, 0):
                remote(slot, c, part, mate, 2).wait_recv()
        for core in range(2):
            @pl.when(c == core)
            def _():
                for axis, sign, part in forwards(core, dz, dy):
                    remote(slot, core, part, near[axis, sign], part).start()
        for part in range(2):
            remote(slot, c, part, mate, 2).start()

    take(*ORDER[0])

    for h in range(4):
        q_scr[h * 128 : (h + 1) * 128, :] = turn(
            q_in[:, h * 128 : (h + 1) * 128], qg[...]
        ).astype(jnp.bfloat16)
    m_scr[...] = jnp.full((512, 128), -1e30, jnp.float32)
    l_scr[...] = jnp.zeros((512, 128), jnp.float32)
    acc[...] = jnp.zeros((512, 128), jnp.float32)
    scale = math.log2(math.e) / math.sqrt(HEAD_SIZE)

    def step(i, carry):
        for k in range(1, 32):
            @pl.when(i == k - 1)
            def _():
                take(*ORDER[k])
        slot = slot_at(*ORDER[0])
        for k in range(1, 32):
            slot = jnp.where(i == k, slot_at(*ORDER[k]), slot)
        for part in range(2):
            remote(slot, 1 - c, part, mate, 2).wait_recv()
        kt = jnp.concatenate([kv[slot, 0, 0], kv[slot, 1, 0]], axis=1)
        vv = jnp.concatenate([kv[slot, 0, 1], kv[slot, 1, 1]], axis=0)
        s = jnp.dot(q_scr[...], kt, preferred_element_type=jnp.float32)
        before = m_scr[...]
        now = jnp.maximum(before, jnp.max(s, axis=1, keepdims=True))
        m_scr[...] = now
        shrink = jnp.exp2((before - now) * scale)
        p = jnp.exp2((s - jnp.concatenate([now, now], axis=1)) * scale)
        l_scr[...] = l_scr[...] * shrink + (p[:, :128] + p[:, 128:])
        acc[...] = acc[...] * shrink + jnp.dot(
            p.astype(jnp.bfloat16), vv, preferred_element_type=jnp.float32
        )
        return carry

    lax.fori_loop(0, 32, step, 0)

    total = jnp.sum(l_scr[...], axis=1, keepdims=True)
    att = (acc[...] / total).astype(jnp.bfloat16)
    att = jnp.concatenate([att[h * 128 : (h + 1) * 128, :] for h in range(4)], axis=1)
    wcopy.wait()
    proj = jnp.dot(att, outw[...], preferred_element_type=jnp.float32).astype(jnp.bfloat16)
    part_out[...] = proj.reshape(4, 32, 2048)

    def cross(k):
        to = (t + k) % 4
        return pltpu.make_async_remote_copy(
            src_ref=part_out.at[to],
            dst_ref=part_in.at[k - 1],
            send_sem=xs_sem.at[k - 1],
            recv_sem=xr_sem.at[k - 1],
            device_id=(me, to),
            device_id_type=MESH,
        )

    for k in (2, 1, 3):
        cross(k).start()
    state = resid[...].astype(jnp.float32) + part_out[t].astype(jnp.float32)
    for k in (1, 3, 2):
        cross(k).wait_recv()
        state = state + part_in[k - 1].astype(jnp.float32)
    state_out[...] = state
    normed_out[...] = (
        state * lax.rsqrt(jnp.mean(state * state, axis=-1, keepdims=True) + norm_eps) * ng[...]
    ).astype(jnp.bfloat16)
    for k in range(1, 4):
        cross(k).wait_send()
    for part in range(2):
        sent = kv.at[0:31, 0, part]
        pltpu.make_async_copy(sent, sent, send_sem.at[part]).wait()
    pltpu.make_async_copy(kv.at[0:16], kv.at[0:16], send_sem.at[2]).wait()


def attend(queries, keys, values, query_gain, key_norm_gain, out_weight, residual, norm_gain):
    inverse = (theta_base ** (-np.arange(32, dtype=np.float64) * 2.0 / 64)).astype(np.float32)
    row = 2 * lax.axis_index("sp") + jnp.arange(2, dtype=jnp.int32)
    by_row = jnp.tile(row.astype(jnp.float32)[:, None] * inverse, (1, 4))
    rowtab = jnp.concatenate([jnp.cos(by_row), jnp.sin(by_row)], axis=0)
    by_col = np.tile(np.arange(64, dtype=np.float32)[:, None] * inverse, (1, 4))
    colcos = jnp.asarray(np.cos(by_col.astype(np.float64)).astype(np.float32))
    colsin = jnp.asarray(np.sin(by_col.astype(np.float64)).astype(np.float32))
    vm = pl.BlockSpec(memory_space=pltpu.VMEM)
    return pl.pallas_call(
        attend_kernel,
        out_shape=(
            jax.ShapeDtypeStruct((32, 2048), jnp.float32),
            jax.ShapeDtypeStruct((32, 2048), jnp.bfloat16),
        ),
        in_specs=[vm] * 8 + [pl.BlockSpec(memory_space=pl.ANY)] + [vm] * 2,
        out_specs=(vm, vm),
        scratch_shapes=[
            pltpu.VMEM((32, 2, 2, 128, 128), jnp.bfloat16),
            pltpu.VMEM((512, 128), jnp.bfloat16),
            pltpu.VMEM((512, 128), jnp.float32),
            pltpu.VMEM((512, 128), jnp.float32),
            pltpu.VMEM((512, 128), jnp.float32),
            pltpu.VMEM((512, 2048), jnp.bfloat16),
            pltpu.VMEM((4, 32, 2048), jnp.bfloat16),
            pltpu.VMEM((3, 32, 2048), jnp.bfloat16),
            pltpu.SemaphoreType.DMA((3,)),
            pltpu.SemaphoreType.DMA((32, 2, 2)),
            pltpu.SemaphoreType.DMA,
            pltpu.SemaphoreType.DMA((3,)),
            pltpu.SemaphoreType.DMA((3,)),
        ],
        compiler_params=pltpu.CompilerParams(
            collective_id=0, has_side_effects=True, vmem_limit_bytes=40 * 1024 * 1024
        ),
        name="attend",
    )(
        queries, keys, values, query_gain.reshape(1, -1), key_norm_gain.reshape(1, -1),
        rowtab, colcos, colsin, out_weight, residual, norm_gain.reshape(1, -1),
    )


def sent_collect(value, axis, dim):
    size = lax.axis_size(axis)
    pieces = lax.all_to_all(
        jnp.broadcast_to(value[None], (size, *value.shape)), axis, 0, 0, tiled=True
    )
    dims = list(pieces.shape[1:])
    dims[dim] *= pieces.shape[0]
    return jnp.moveaxis(pieces, 0, dim).reshape(dims)


def on_device(
    queries,
    keys,
    values,
    query_gain,
    key_norm_gain,
    out_weight,
    residual,
    norm_gain,
    expert_gate,
    expert_up,
    expert_down,
    routes,
    route_weight,
):
    local_rows = queries.shape[0]
    out_rows, model_width = residual.shape
    hidden_state, normed = attend(
        queries, keys, values, query_gain, key_norm_gain, out_weight, residual, norm_gain
    )
    route_top = routes.shape[1]
    group_width = lax.axis_size("tp")
    expert_count = lax.axis_size("sp") * expert_gate.shape[0]
    capacity = 2 * max(1, route_top * local_rows // (group_width * expert_count))
    flat_routes = routes.reshape(-1)
    onehot = (flat_routes[:, None] == jnp.arange(expert_count, dtype=jnp.int32)[None, :]).astype(
        jnp.int32
    )
    earlier = jnp.cumsum(onehot, axis=0) - onehot
    slot_rank = jnp.sum(earlier * onehot, axis=1)
    slot_index = flat_routes * capacity + slot_rank
    placer = (
        jnp.arange(expert_count * capacity, dtype=jnp.int32)[:, None] == slot_index[None, :]
    ).astype(jnp.bfloat16)
    route_rows = jnp.repeat(normed, route_top, axis=0)
    buffer = jnp.dot(placer, route_rows, preferred_element_type=jnp.float32).astype(jnp.bfloat16)
    buffer = buffer.reshape(expert_count, capacity, model_width)
    mail_rows = lax.all_to_all(buffer, "sp", split_axis=0, concat_axis=0, tiled=True)
    inbox_rows = sent_collect(mail_rows, "tp", 1)
    source_count = inbox_rows.shape[0]
    rows_in = inbox_rows.reshape(-1, model_width)
    gate_proj = jnp.dot(rows_in, expert_gate[0], preferred_element_type=jnp.float32)
    up_proj = jnp.dot(rows_in, expert_up[0], preferred_element_type=jnp.float32)
    hidden_act = (jax.nn.silu(gate_proj) * up_proj).astype(jnp.bfloat16)
    down_part = jnp.dot(hidden_act, expert_down[0], preferred_element_type=jnp.float32)
    down_part = down_part.reshape(source_count, group_width * capacity, model_width)
    summed = lax.psum_scatter(down_part.astype(jnp.bfloat16), "tp", scatter_dimension=1, tiled=True)
    returned = lax.all_to_all(summed, "sp", split_axis=0, concat_axis=0, tiled=True)
    per_route = jnp.dot(
        placer.T, returned.reshape(-1, model_width), preferred_element_type=jnp.float32
    )
    per_route = per_route.reshape(out_rows, route_top, model_width)
    moe_sum = jnp.sum(route_weight[:, :, None] * per_route, axis=1)
    return (hidden_state + moe_sum).astype(jnp.bfloat16)


def solution(mesh):
    placed = (
        P("sp", "tp"),
        P("sp", "tp"),
        P("sp", "tp"),
        P(),
        P(),
        P("tp", None),
        P(("sp", "tp"), None),
        P(),
        P("sp", None, "tp"),
        P("sp", None, "tp"),
        P("sp", "tp", None),
        P(("sp", "tp"), None),
        P(("sp", "tp"), None),
    )
    return jax.shard_map(
        on_device, mesh=mesh, in_specs=placed, out_specs=P(("sp", "tp"), None), check_vma=False
    )
```

time: 368 us -> 240 us (0.65)
  waiting for transfers between devices: 124 us -> 45.4 us
  Pallas kernels: 0 us -> 66.6 us
  matrix products: 80.3 us -> 17 us
  other arithmetic: 32.9 us -> 2.06 us
  local copies, waits for them, and re-layouts: 43.1 us -> 31.3 us
  starting transfers between devices: 15.1 us -> 10.9 us
    all_gather x1 -> x0, waiting for transfers between devices: 71.9 us -> none  [in_one_piece(): lax.all_gather(both, axis, axis=dim, tiled=True)]
    pallas_call x0 -> x1, Pallas kernels: none -> 66.6 us  [attend(): pl.pallas_call(attend_kernel, out_shape=(jax.ShapeDtypeStruct((32, 2048),...]
    dot_general x33 -> x0, matrix products: 63.3 us -> none  [the longest x16 34.9 us: one_span(): jnp.einsum('hqd,khd->hqk', query_block, key_span, preferred_element_type=...]
    reduce_sum x20 -> x0, other arithmetic: 23.9 us -> none  [the longest x16 22.6 us: one_span(): norm_sum = norm_sum * shrink + jnp.sum(weights, axis=-1)]
    slice x3 -> x0, local copies, waits for them, and re-layouts: 12.8 us -> none  [in_one_piece(): lax.slice_in_dim(result, at, at + a.shape[along], axis=along)]
    all_to_all x1 -> x0, waiting for transfers between devices: 8.81 us -> none  [sent_and_summed(): lax.all_to_all(pieces, axis, split_axis=0, concat_axis=0, tiled=True)]
    unnamed x12 -> x27, local copies, waits for them, and re-layouts: 4.29 us -> 8.53 us
    all_to_all x1 -> x0, starting transfers between devices: 4.13 us -> none  [sent_and_summed(): lax.all_to_all(pieces, axis, split_axis=0, concat_axis=0, tiled=True)]
  transfers between devices with their start and end apart: 4 -> 2, of which waited for: 4 -> 2; matrix products, arithmetic and copies ran while one was open for 3% -> 0% of each run, Pallas kernels for 0% -> 0%
where the time goes in v1:
time: 240 us; the launch traced here: 239 us
  Pallas kernels  66.6 us (28%)
  blocking collectives  52.2 us (22%)
  waiting for transfers between devices  45.4 us (19%)
  local copies, waits for them, and re-layouts  31.3 us (13%)
  matrix products  17 us (7%)
  between operations  13.5 us (6%)
  starting transfers between devices  10.9 us (5%)
    pallas_call x1, Pallas kernels, attend(): pl.pallas_call(attend_kernel, out_shape=(jax.ShapeDtypeStruct((32, 2048),...  66.6 us
    all_to_all x1, blocking collectives, sent_collect(): lax.all_to_all(jnp.broadcast_to(value[None], (size, *value.shape)), axis,...  28.3 us
    reduce_scatter x1, waiting for transfers between devices, on_device(): lax.psum_scatter(down_part.astype(jnp.bfloat16), 'tp', scatter_dimension=...  27.9 us
    all_to_all x1, blocking collectives, on_device(): lax.all_to_all(buffer, 'sp', split_axis=0, concat_axis=0, tiled=True)  23.8 us
    all_to_all x1, waiting for transfers between devices, on_device(): lax.all_to_all(summed, 'sp', split_axis=0, concat_axis=0, tiled=True)  17.5 us
    all_to_all x1, starting transfers between devices, on_device(): lax.all_to_all(summed, 'sp', split_axis=0, concat_axis=0, tiled=True)  10.9 us
    unnamed x27, local copies, waits for them, and re-layouts  8.53 us
    dot_general x1, matrix products, on_device(): jnp.dot(hidden_act, expert_down[0], preferred_element_type=jnp.float32)  8.22 us
  transfers between devices with their start and end apart: 2, of which 2 were waited for; matrix products, arithmetic and copies ran while one was open for 0% of the time, Pallas kernels for 0%

profile of v1, /device:TPU:1, one launch (start us, length us, event | category | flops | bytes accessed | tf_op | source)
XLA Modules:
  0.0 239.0 jit_solution(16943474740366838713)
XLA Ops:
  6.5 0.9 multiply_cosine_fusion
  7.7 1.6 copy-done.1
  9.3 0.9 copy-done.2
  10.2 0.9 copy-done.3
  12.6 0.8 copy-done.6
  16.1 66.6 %attend.1 = (f32[32,2048]{1,0:T(8,128)S(1)}, bf16[32,2048]{1,0:T(8,128)(2,1)S(1)}) custom-call(bf16[128,512]{1,0:T(8,128)(2,1)S(1)} %copy-done.2, bf16[128,128]{1,0:T(8,128)(2,1)S(1)} %copy-done.4, bf16[128,128]{1,0:T(8,128)(2,1)S(1)} %copy-done.5, f32[1,128]{1,0:T(1,128)S(1)} %bitcast.31, f32[1,128]{1,0:T(1,128)S(1)} %bitcast.32, ...), custom_call_target="tpu_custom_call" | custom-call | tf_op jit(solution)/shard_map/attend/pallas_call | solution.py:228
  82.8 0.8 broadcast_in_dim.4
  83.6 1.8 reshape.100
  85.9 2.0 convolution_convert_fusion
  88.0 2.2 reshape.101
  90.1 23.8 %all_to_all.15 = bf16[64,2,2048]{2,1,0:T(2,128)(2,1)S(1)} all-to-all(bf16[64,2,2048]{2,1,0:T(2,128)(2,1)} %reshape.101), channel_id=1, replica_groups=mesh['sp'=64,'tp'=4] {'sp'}, dimensions={0} | all-to-all | bytes 1048576 | tf_op jit(solution)/shard_map/all_to_all | solution.py:308
  114.0 1.3 broadcast_in_dim.5
  115.3 28.3 %all_to_all.16 = bf16[4,64,2,2048]{3,2,1,0:T(2,128)(2,1)S(1)} all-to-all(bf16[4,64,2,2048]{3,2,1,0:T(2,128)(2,1)S(1)} %broadcast_in_dim.5), channel_id=1, replica_groups=mesh['sp'=64,'tp'=4] {'tp'}, dimensions={0} | all-to-all | bytes 4194304 | tf_op jit(solution)/shard_map/all_to_all | solution.py:263
  143.6 3.8 %copy.26 = bf16[64,4,2,2048]{3,2,1,0:T(2,128)(2,1)} copy(bf16[64,4,2,2048]{3,2,0,1:T(2,128)(2,1)S(1)} %bitcast.33) | data formatting | bytes 4194304 | tf_op jit(solution)/shard_map/transpose | solution.py:268
  147.4 4.1 %reshape_reshape.3 = bf16[512,2048]{1,0:T(8,128)(2,1)} reshape(bf16[64,4,2,2048]{3,2,1,0:T(2,128)(2,1)} %copy.26) | data formatting | bytes 4194304 | tf_op jit(solution)/shard_map/reshape;reshape | solution.py:311
  151.5 5.5 %fusion.4 = f32[512,768]{1,0:T(8,128)} fusion(bf16[512,2048]{1,0:T(8,128)(2,1)} %reshape_reshape.3, bf16[1,2048,768]{2,1,0:T(8,128)(2,1)} %param.24), kind=kOutput, calls=%fused_computation.4 | convolution fusion | flops 1610612736 | bytes 6815744 | tf_op jit(solution)/shard_map/dot_general | solution.py:312
  157.0 8.2 %fusion.6 = bf16[64,8,2048]{2,1,0:T(8,128)(2,1)} fusion(bf16[1,768,2048]{2,1,0:T(8,128)(2,1)S(1)} %copy-done, bf16[512,2048]{1,0:T(8,128)(2,1)} %reshape_reshape.3, bf16[1,2048,768]{2,1,0:T(8,128)(2,1)} %param.25, f32[512,768]{1,0:T(8,128)} %fusion.4), kind=kOutput, calls=%fused_computation.6 | convolution fusion | flops 3224633344 | bytes 12058624 | tf_op jit(solution)/shard_map/dot_general | solution.py:315
  165.2 4.1 %copy.27 = bf16[64,8,2048]{2,0,1:T(8,128)(2,1)} copy(bf16[64,8,2048]{2,1,0:T(8,128)(2,1)} %fusion.6) | data formatting | bytes 4194304 | tf_op jit(solution)/shard_map/convert_element_type | solution.py:317
  169.3 27.9 %reduce-scatter.2.cloned.1.call-done = bf16[64,2,2048]{2,0,1:T(8,128)(2,1)} async-done(((bf16[64,8,2048]{2,0,1:T(8,128)(2,1)}), bf16[64,2,2048]{2,0,1:T(8,128)(2,1)}) %reduce-scatter.2.cloned.1.call-update) | async-done | bytes 524304 | tf_op jit(solution)/shard_map/reduce_scatter | solution.py:317
  197.2 2.4 copy.28
  199.6 10.9 %all-to-all-start.2 = ((bf16[64,2,2048]{2,1,0:T(2,128)(2,1)}), bf16[64,2,2048]{2,1,0:T(2,128)(2,1)}, u32[]{:S(2)}, u32[]{:S(2)}) async-start(bf16[64,2,2048]{2,1,0:T(2,128)(2,1)} %copy.28), calls=%async_computation.3 | async-start | bytes 1048576 | tf_op jit(solution)/shard_map/all_to_all | solution.py:318
  210.6 17.5 %all-to-all-done.2 = bf16[64,2,2048]{2,1,0:T(2,128)(2,1)} async-done(((bf16[64,2,2048]{2,1,0:T(2,128)(2,1)}), bf16[64,2,2048]{2,1,0:T(2,128)(2,1)}, u32[]{:S(2)}, u32[]{:S(2)}) %all-to-all-start.2) | async-done | bytes 524320 | tf_op jit(solution)/shard_map/all_to_all | solution.py:318
  228.1 2.0 reshape.104
  230.1 1.3 fusion.14
  (39 shorter events, 5.8 us)
Async XLA Ops:
  6.5 150.4 %copy-start = (bf16[1,768,2048]{2,1,0:T(8,128)(2,1)S(1)}, bf16[1,768,2048]{2,1,0:T(8,128)(2,1)}, u32[]{:S(2)}) copy-start(bf16[1,768,2048]{2,1,0:T(8,128)(2,1)} %param.26) | copy-start | bytes 9437188
  6.5 78.8 %copy-start.12 = (s32[32,2]{0,1:T(2,128)S(1)}, s32[32,2]{0,1:T(2,128)}, u32[]{:S(2)}) copy-start(s32[32,2]{0,1:T(2,128)} %param.27) | copy-start | bytes 772
  6.5 190.6 %reduce-scatter.2.cloned.1.call-start = ((), (), s32[]{:S(2)}) async-start(), calls=%async_computation.4 | async-start | bytes 2621440 | tf_op jit(solution)/shard_map/reduce_scatter | solution.py:317
  7.7 1.6 copy-start.1
  9.3 0.9 copy-start.2
  10.2 0.9 copy-start.3
  11.1 0.8 copy-start.4
  11.8 0.8 copy-start.5
  12.6 0.8 copy-start.6
  13.3 0.8 copy-start.7
  14.1 0.7 copy-start.8
  14.8 0.7 copy-start.9
  15.5 0.7 copy-start.10
  169.3 60.8 %copy-start.11 = (f32[32,2]{0,1:T(2,128)S(1)}, f32[32,2]{0,1:T(2,128)}, u32[]{:S(2)}) copy-start(f32[32,2]{0,1:T(2,128)} %param.28) | copy-start | bytes 772
  199.6 28.5 %all-to-all-start.2 = ((bf16[64,2,2048]{2,1,0:T(2,128)(2,1)}), bf16[64,2,2048]{2,1,0:T(2,128)(2,1)}, u32[]{:S(2)}, u32[]{:S(2)}) async-start(bf16[64,2,2048]{2,1,0:T(2,128)(2,1)} %copy.28), calls=%async_computation.3 | async-start | bytes 1048576 | tf_op jit(solution)/shard_map/all_to_all | solution.py:318
Sparse Core Ops, SparseCore 0:
  169.4 27.7 reduce-scatter.1

commit v2 on v1

--- a/solution.py
+++ b/solution.py
@@ -59,16 +59,29 @@
 
 
 def attend_kernel(
-    q_in, k_in, v_in, qg, kg, rowtab, colcos, colsin, outw_hbm, resid, ng,
+    q_hbm, k_hbm, v_hbm, qg_hbm, kg_hbm, rowtab_hbm, colcos_hbm, colsin_hbm, outw_hbm, resid_hbm, ng_hbm,
     state_out, normed_out,
+    q_in, k_in, v_in, qg, kg, rowtab, colcos, colsin, resid, ng,
     kv, q_scr, m_scr, l_scr, acc, outw, part_out, part_in,
-    send_sem, recv_sem, w_sem, xs_sem, xr_sem,
+    in_sem, send_sem, recv_sem, w_sem, xs_sem, xr_sem,
 ):
     me = lax.axis_index("sp")
     t = lax.axis_index("tp")
     z, y, c = me // 8, (me // 2) % NY, me % 2
     chip = me // 2
 
+    fetch = [
+        pltpu.make_async_copy(s, d, in_sem.at[i])
+        for i, (s, d) in enumerate(
+            [
+                (k_hbm, k_in), (kg_hbm, kg), (rowtab_hbm, rowtab), (colcos_hbm, colcos),
+                (colsin_hbm, colsin), (v_hbm, v_in), (q_hbm, q_in), (qg_hbm, qg),
+                (resid_hbm, resid), (ng_hbm, ng),
+            ]
+        )
+    ]
+    for cp in fetch:
+        cp.start()
     wcopy = pltpu.make_async_copy(outw_hbm, outw, w_sem)
     wcopy.start()
 
@@ -89,6 +102,8 @@
     for k in range(1, 4):
         pl.semaphore_signal(barrier, inc=1, device_id=(me, (t + k) % 4), device_id_type=MESH)
 
+    for cp in fetch[:6]:
+        cp.wait()
     lane = lax.broadcasted_iota(jnp.int32, (64, 128), 1)
     low = lane < 64
 
@@ -144,6 +159,8 @@
             remote(slot, c, part, mate, 2).start()
 
     take(*ORDER[0])
+    for cp in fetch[6:]:
+        cp.wait()
 
     for h in range(4):
         q_scr[h * 128 : (h + 1) * 128, :] = turn(
@@ -231,9 +248,19 @@
             jax.ShapeDtypeStruct((32, 2048), jnp.float32),
             jax.ShapeDtypeStruct((32, 2048), jnp.bfloat16),
         ),
-        in_specs=[vm] * 8 + [pl.BlockSpec(memory_space=pl.ANY)] + [vm] * 2,
+        in_specs=[pl.BlockSpec(memory_space=pl.ANY)] * 11,
         out_specs=(vm, vm),
         scratch_shapes=[
+            pltpu.VMEM((128, 512), jnp.bfloat16),
+            pltpu.VMEM((128, 128), jnp.bfloat16),
+            pltpu.VMEM((128, 128), jnp.bfloat16),
+            pltpu.VMEM((1, 128), jnp.float32),
+            pltpu.VMEM((1, 128), jnp.float32),
+            pltpu.VMEM((4, 128), jnp.float32),
+            pltpu.VMEM((64, 128), jnp.float32),
+            pltpu.VMEM((64, 128), jnp.float32),
+            pltpu.VMEM((32, 2048), jnp.bfloat16),
+            pltpu.VMEM((1, 2048), jnp.float32),
             pltpu.VMEM((32, 2, 2, 128, 128), jnp.bfloat16),
             pltpu.VMEM((512, 128), jnp.bfloat16),
             pltpu.VMEM((512, 128), jnp.float32),
@@ -242,6 +269,7 @@
             pltpu.VMEM((512, 2048), jnp.bfloat16),
             pltpu.VMEM((4, 32, 2048), jnp.bfloat16),
             pltpu.VMEM((3, 32, 2048), jnp.bfloat16),
+            pltpu.SemaphoreType.DMA((10,)),
             pltpu.SemaphoreType.DMA((3,)),
             pltpu.SemaphoreType.DMA((32, 2, 2)),
             pltpu.SemaphoreType.DMA,
@@ -258,14 +286,383 @@
     )
 
 
-def sent_collect(value, axis, dim):
-    size = lax.axis_size(axis)
-    pieces = lax.all_to_all(
-        jnp.broadcast_to(value[None], (size, *value.shape)), axis, 0, 0, tiled=True
+def perm_pair():
+    row = lax.broadcasted_iota(jnp.int32, (256, 256), 0)
+    col = lax.broadcasted_iota(jnp.int32, (256, 256), 1)
+    to_blocks = (((row // 2) % 16) * 16 + (row // 32) * 2 + row % 2) == col
+    to_rows = (((col // 2) % 16) * 16 + (col // 32) * 2 + col % 2) == row
+    return (
+        jnp.where(to_blocks, 1.0, 0.0).astype(jnp.bfloat16),
+        jnp.where(to_rows, 1.0, 0.0).astype(jnp.bfloat16),
     )
-    dims = list(pieces.shape[1:])
-    dims[dim] *= pieces.shape[0]
-    return jnp.moveaxis(pieces, 0, dim).reshape(dims)
+
+
+def moved(perm, value):
+    return jnp.dot(perm, value, preferred_element_type=jnp.float32).astype(jnp.bfloat16)
+
+
+def experts_kernel(
+    normed_hbm, state_hbm, rrow_hbm, rcol_hbm, rw_hbm, wg_hbm, wu_hbm, wd_hbm,
+    out,
+    normed, state, rrow, rcol, rw, wg, wu, wd,
+    sb, xb, rows, hid, down, relay_in, relay_out, final_in, ob, cb,
+    in_sem, w_sem, a_send, a_recv, x_send, x_recv, r_send, r_recv, b_send, b_recv,
+):
+    me = lax.axis_index("sp")
+    t = lax.axis_index("tp")
+    z = me // 8
+    right, left = (t + 1) % 4, (t + 3) % 4
+    far = (t + 2) % 4
+
+    small = [
+        pltpu.make_async_copy(s, d, in_sem.at[i])
+        for i, (s, d) in enumerate(
+            [(normed_hbm, normed), (rrow_hbm, rrow), (rcol_hbm, rcol), (rw_hbm, rw), (state_hbm, state)]
+        )
+    ]
+    weights = [
+        pltpu.make_async_copy(s, d, w_sem.at[i])
+        for i, (s, d) in enumerate([(wg_hbm.at[0], wg), (wu_hbm.at[0], wu), (wd_hbm.at[0], wd)])
+    ]
+    for cp in small + weights:
+        cp.start()
+
+    barrier = pltpu.get_barrier_semaphore()
+
+    def hello(k, carry):
+        pl.semaphore_signal(
+            barrier, inc=1, device_id=((me + k) % 64, t), device_id_type=MESH
+        )
+        return carry
+
+    lax.fori_loop(1, 64, hello, 0)
+    for peer in (right, left):
+        pl.semaphore_signal(barrier, inc=1, device_id=(me, peer), device_id_type=MESH)
+
+    to_blocks, to_rows = perm_pair()
+
+    for cp in small:
+        cp.wait()
+    same = rcol[...] == rrow[...]
+    sub = lax.broadcasted_iota(jnp.int32, (64, 64), 0)
+    lane = lax.broadcasted_iota(jnp.int32, (64, 64), 1)
+    slot_row = rrow[...] * 2 + jnp.sum(
+        jnp.where(same & (sub < lane), 1, 0), axis=0, keepdims=True
+    )
+    slot_col = rcol[...] * 2 + jnp.sum(
+        jnp.where(same & (lane < sub), 1, 0), axis=1, keepdims=True
+    )
+    place = lax.broadcasted_iota(jnp.int32, (128, 32), 0)
+    placer = (
+        jnp.where(place == slot_row[:, :32], 1.0, 0.0)
+        + jnp.where(place == slot_row[:, 32:], 1.0, 0.0)
+    ).astype(jnp.bfloat16)
+    picker = jnp.where(
+        lax.broadcasted_iota(jnp.int32, (64, 128), 1) == slot_col, 1.0, 0.0
+    ).astype(jnp.bfloat16)
+    mail = moved(placer, normed[...])
+
+    def stacked(value):
+        return jnp.concatenate(
+            [value[:, ct * 128 : (ct + 1) * 128] for ct in range(16)], axis=0
+        )
+
+    for g in range(0, 8, 2):
+        pair = jnp.concatenate(
+            [stacked(mail[16 * g : 16 * g + 16]), stacked(mail[16 * g + 16 : 16 * g + 32])], axis=1
+        )
+        pair = moved(to_blocks, pair)
+        sb[8 * g : 8 * g + 8] = pair[:, :128].reshape(8, 32, 128)
+        sb[8 * g + 8 : 8 * g + 16] = pair[:, 128:].reshape(8, 32, 128)
+
+    def zone(u):
+        return (z + 8 + ((u + 1) // 2) * (2 * (u % 2) - 1)) % 8
+
+    xb[t, me] = sb[me]
+    pl.semaphore_wait(barrier, 65)
+
+    def post(k, carry):
+        u, i = k // 8, k % 8
+        to = zone(u) * 8 + (me + i) % 8
+
+        @pl.when(k > 0)
+        def _():
+            pltpu.make_async_remote_copy(
+                src_ref=sb.at[to],
+                dst_ref=xb.at[t, me],
+                send_sem=a_send,
+                recv_sem=a_recv.at[z],
+                device_id=(to, t),
+                device_id_type=MESH,
+            ).start()
+
+        return carry
+
+    lax.fori_loop(0, 64, post, 0)
+
+    def local_wait(ref, sem):
+        pltpu.make_async_copy(ref, ref, sem).wait()
+
+    def spread(u, block, lo, n, lane_id, peer):
+        src = xb.at[block, pl.ds(zone(u) * 8 + lo, n)]
+        return pltpu.make_async_remote_copy(
+            src_ref=src,
+            dst_ref=src,
+            send_sem=x_send.at[u, lane_id],
+            recv_sem=x_recv.at[u, lane_id],
+            device_id=(me, peer),
+            device_id_type=MESH,
+        )
+
+    def spread_all(u):
+        return (
+            spread(u, t, 0, 8, 0, right),
+            spread(u, t, 0, 8, 1, left),
+            spread(u, left, 0, 4, 2, right),
+            spread(u, right, 4, 4, 3, left),
+        )
+
+    def arrivals(u):
+        return (
+            spread(u, left, 0, 8, 0, right),
+            spread(u, right, 0, 8, 1, left),
+            spread(u, far, 0, 4, 2, right),
+            spread(u, far, 4, 4, 3, left),
+        )
+
+    def dispatch(i, carry):
+        @pl.when(i == 0)
+        def _():
+            local_wait(xb.at[t, 0:7], a_recv.at[z])
+
+        @pl.when((i > 0) & (i < 8))
+        def _():
+            local_wait(xb.at[t, 0:8], a_recv.at[zone(i)])
+
+        @pl.when(i < 8)
+        def _():
+            for cp in spread_all(i)[:2]:
+                cp.start()
+
+        @pl.when((i > 0) & (i < 9))
+        def _():
+            for k in range(2):
+                arrivals(i - 1)[k].wait_recv()
+                spread_all(i - 1)[2 + k].start()
+
+        @pl.when(i > 1)
+        def _():
+            u = i - 2
+            for k in range(2):
+                arrivals(u)[2 + k].wait_recv()
+            zi = zone(u)
+            at = pl.multiple_of(zi * 16, 16)
+            for h in range(0, 4, 2):
+                pair = jnp.concatenate(
+                    [xb[h + d, pl.ds(zi * 8, 8)].reshape(256, 128) for d in range(2)], axis=1
+                )
+                pair = moved(to_rows, pair)
+                for d in range(2):
+                    for ct in range(16):
+                        rows[h + d, pl.ds(at, 16), ct * 128 : (ct + 1) * 128] = pair[
+                            ct * 16 : ct * 16 + 16, d * 128 : (d + 1) * 128
+                        ]
+
+        return carry
+
+    lax.fori_loop(0, 10, dispatch, 0)
+
+    for cp in weights[:2]:
+        cp.wait()
+
+    def gate_up(n, carry):
+        cols = pl.ds(pl.multiple_of(n * 256, 256), 256)
+        x = rows[...].reshape(512, 2048)
+        gate = jnp.dot(x, wg[:, cols], preferred_element_type=jnp.float32)
+        up = jnp.dot(x, wu[:, cols], preferred_element_type=jnp.float32)
+        hid[:, cols] = (gate / (1.0 + jnp.exp(-gate)) * up).astype(jnp.bfloat16)
+        return carry
+
+    lax.fori_loop(0, 3, gate_up, 0)
+    weights[2].wait()
+
+    def down_tile(n, carry):
+        cols = pl.ds(pl.multiple_of(n * 256, 256), 256)
+        d = jnp.dot(hid[...], wd[:, cols], preferred_element_type=jnp.float32)
+        down[:, :, cols] = d.astype(jnp.bfloat16).reshape(4, 128, 256)
+        return carry
+
+    lax.fori_loop(0, 8, down_tile, 0)
+
+    lo, hi = pl.ds(0, 1024), pl.ds(1024, 1024)
+
+    def ring(u, src, dst, lane_id, peer):
+        return pltpu.make_async_remote_copy(
+            src_ref=src,
+            dst_ref=dst,
+            send_sem=r_send.at[u, lane_id],
+            recv_sem=r_recv.at[u, lane_id],
+            device_id=(me, peer),
+            device_id_type=MESH,
+        )
+
+    def piece(block, u, half):
+        return down.at[block, pl.ds(pl.multiple_of(zone(u) * 16, 16), 16), half]
+
+    def first_sends(u):
+        return (
+            ring(u, piece(far, u, lo), relay_in.at[0, u], 0, right),
+            ring(u, piece(far, u, hi), relay_in.at[1, u], 1, left),
+            ring(u, piece(right, u, hi), final_in.at[0, u, :, hi], 2, right),
+            ring(u, piece(left, u, lo), final_in.at[1, u, :, lo], 3, left),
+        )
+
+    def second_sends(u):
+        return (
+            ring(u, relay_out.at[0, u], final_in.at[0, u, :, lo], 4, right),
+            ring(u, relay_out.at[1, u], final_in.at[1, u, :, hi], 5, left),
+        )
+
+    def back(u, i):
+        to = zone(u) * 8 + (me + i) % 8
+        return pltpu.make_async_remote_copy(
+            src_ref=ob.at[to],
+            dst_ref=cb.at[me],
+            send_sem=b_send,
+            recv_sem=b_recv,
+            device_id=(to, t),
+            device_id_type=MESH,
+        )
+
+    def combine(i, carry):
+        @pl.when(i < 8)
+        def _():
+            for cp in first_sends(7 - i):
+                cp.start()
+
+        @pl.when((i > 0) & (i < 9))
+        def _():
+            u = 8 - i
+            for k, (block, half) in enumerate(((right, lo), (left, hi))):
+                first_sends(u)[k].wait_recv()
+                at = pl.ds(pl.multiple_of(zone(u) * 16, 16), 16)
+                relay_out[k, u] = (
+                    relay_in[k, u].astype(jnp.float32) + down[block, at, half].astype(jnp.float32)
+                ).astype(jnp.bfloat16)
+                second_sends(u)[k].start()
+
+        @pl.when(i > 1)
+        def _():
+            u = 9 - i
+            for cp in first_sends(u)[2:] + second_sends(u):
+                cp.wait_recv()
+            zi = zone(u)
+            at = pl.ds(pl.multiple_of(zi * 16, 16), 16)
+            whole = (
+                down[t, at, :].astype(jnp.float32)
+                + final_in[0, u].astype(jnp.float32)
+                + final_in[1, u].astype(jnp.float32)
+            ).astype(jnp.bfloat16)
+            ob[pl.ds(zi * 8, 8)] = moved(to_blocks, stacked(whole)).reshape(8, 32, 128)
+
+            @pl.when(u == 0)
+            def _():
+                cb[me] = ob[me]
+
+            for k in range(8):
+                if k == 0:
+                    @pl.when(u > 0)
+                    def _():
+                        back(u, 0).start()
+                else:
+                    back(u, k).start()
+
+        return carry
+
+    lax.fori_loop(0, 10, combine, 0)
+
+    local_wait(cb.at[0:63], b_recv)
+    nat = []
+    for g in range(0, 8, 2):
+        pair = jnp.concatenate(
+            [cb[8 * g + 8 * d : 8 * g + 8 * d + 8].reshape(256, 128) for d in range(2)], axis=1
+        )
+        pair = moved(to_rows, pair)
+        for d in range(2):
+            nat.append(
+                jnp.concatenate(
+                    [
+                        pair[ct * 16 : ct * 16 + 16, d * 128 : (d + 1) * 128]
+                        for ct in range(16)
+                    ],
+                    axis=1,
+                )
+            )
+    nat = jnp.concatenate(nat, axis=0)
+    picked = jnp.dot(picker, nat, preferred_element_type=jnp.float32)
+    out[...] = (
+        state[...] + rw[:, 0:1] * picked[:32] + rw[:, 1:2] * picked[32:]
+    ).astype(jnp.bfloat16)
+
+    local_wait(cb.at[0:63], a_send)
+    local_wait(cb.at[0:63], b_send)
+
+    def drain(u, carry):
+        for cp in spread_all(u) + first_sends(u) + second_sends(u):
+            cp.wait_send()
+        return carry
+
+    lax.fori_loop(0, 8, drain, 0)
+
+
+def experts(normed, state, routes, route_weight, expert_gate, expert_up, expert_down):
+    flat = routes.T.reshape(1, 64)
+    anywhere = pl.BlockSpec(memory_space=pl.ANY)
+    bf16, f32, i32 = jnp.bfloat16, jnp.float32, jnp.int32
+    dma = pltpu.SemaphoreType.DMA
+    return pl.pallas_call(
+        experts_kernel,
+        out_shape=jax.ShapeDtypeStruct((32, 2048), bf16),
+        in_specs=[anywhere] * 8,
+        out_specs=pl.BlockSpec(memory_space=pltpu.VMEM),
+        scratch_shapes=[
+            pltpu.VMEM((32, 2048), bf16),
+            pltpu.VMEM((32, 2048), f32),
+            pltpu.VMEM((1, 64), i32),
+            pltpu.VMEM((64, 1), i32),
+            pltpu.VMEM((32, 2), f32),
+            pltpu.VMEM((2048, 768), bf16),
+            pltpu.VMEM((2048, 768), bf16),
+            pltpu.VMEM((768, 2048), bf16),
+            pltpu.VMEM((64, 32, 128), bf16),
+            pltpu.VMEM((4, 64, 32, 128), bf16),
+            pltpu.VMEM((4, 128, 2048), bf16),
+            pltpu.VMEM((512, 768), bf16),
+            pltpu.VMEM((4, 128, 2048), bf16),
+            pltpu.VMEM((2, 8, 16, 1024), bf16),
+            pltpu.VMEM((2, 8, 16, 1024), bf16),
+            pltpu.VMEM((2, 8, 16, 2048), bf16),
+            pltpu.VMEM((64, 32, 128), bf16),
+            pltpu.VMEM((64, 32, 128), bf16),
+            dma((5,)),
+            dma((3,)),
+            dma,
+            dma((8,)),
+            dma((8, 4)),
+            dma((8, 4)),
+            dma((8, 6)),
+            dma((8, 6)),
+            dma,
+            dma,
+        ],
+        compiler_params=pltpu.CompilerParams(
+            collective_id=1, has_side_effects=True, vmem_limit_bytes=56 * 1024 * 1024
+        ),
+        name="experts",
+    )(
+        normed, state, flat, flat.reshape(64, 1), route_weight,
+        expert_gate, expert_up, expert_down,
+    )
 
 
 def on_device(
@@ -283,45 +680,10 @@
     routes,
     route_weight,
 ):
-    local_rows = queries.shape[0]
-    out_rows, model_width = residual.shape
-    hidden_state, normed = attend(
+    state, normed = attend(
         queries, keys, values, query_gain, key_norm_gain, out_weight, residual, norm_gain
     )
-    route_top = routes.shape[1]
-    group_width = lax.axis_size("tp")
-    expert_count = lax.axis_size("sp") * expert_gate.shape[0]
-    capacity = 2 * max(1, route_top * local_rows // (group_width * expert_count))
-    flat_routes = routes.reshape(-1)
-    onehot = (flat_routes[:, None] == jnp.arange(expert_count, dtype=jnp.int32)[None, :]).astype(
-        jnp.int32
-    )
-    earlier = jnp.cumsum(onehot, axis=0) - onehot
-    slot_rank = jnp.sum(earlier * onehot, axis=1)
-    slot_index = flat_routes * capacity + slot_rank
-    placer = (
-        jnp.arange(expert_count * capacity, dtype=jnp.int32)[:, None] == slot_index[None, :]
-    ).astype(jnp.bfloat16)
-    route_rows = jnp.repeat(normed, route_top, axis=0)
-    buffer = jnp.dot(placer, route_rows, preferred_element_type=jnp.float32).astype(jnp.bfloat16)
-    buffer = buffer.reshape(expert_count, capacity, model_width)
-    mail_rows = lax.all_to_all(buffer, "sp", split_axis=0, concat_axis=0, tiled=True)
-    inbox_rows = sent_collect(mail_rows, "tp", 1)
-    source_count = inbox_rows.shape[0]
-    rows_in = inbox_rows.reshape(-1, model_width)
-    gate_proj = jnp.dot(rows_in, expert_gate[0], preferred_element_type=jnp.float32)
-    up_proj = jnp.dot(rows_in, expert_up[0], preferred_element_type=jnp.float32)
-    hidden_act = (jax.nn.silu(gate_proj) * up_proj).astype(jnp.bfloat16)
-    down_part = jnp.dot(hidden_act, expert_down[0], preferred_element_type=jnp.float32)
-    down_part = down_part.reshape(source_count, group_width * capacity, model_width)
-    summed = lax.psum_scatter(down_part.astype(jnp.bfloat16), "tp", scatter_dimension=1, tiled=True)
-    returned = lax.all_to_all(summed, "sp", split_axis=0, concat_axis=0, tiled=True)
-    per_route = jnp.dot(
-        placer.T, returned.reshape(-1, model_width), preferred_element_type=jnp.float32
-    )
-    per_route = per_route.reshape(out_rows, route_top, model_width)
-    moe_sum = jnp.sum(route_weight[:, :, None] * per_route, axis=1)
-    return (hidden_state + moe_sum).astype(jnp.bfloat16)
+    return experts(normed, state, routes, route_weight, expert_gate, expert_up, expert_down)
 
 
 def solution(mesh):

time: 240 us -> 158 us (0.66)
  Pallas kernels: 66.6 us -> 141 us
  blocking collectives: 52.2 us -> 0 us
  waiting for transfers between devices: 45.4 us -> 0 us
  matrix products: 17 us -> 0 us
  local copies, waits for them, and re-layouts: 31.3 us -> 15.6 us
  between operations: 13.5 us -> 0.05 us
  starting transfers between devices: 10.9 us -> 0 us
    pallas_call x0 -> x1, Pallas kernels: none -> 73.7 us  [experts(): pl.pallas_call(experts_kernel, out_shape=jax.ShapeDtypeStruct((32, 2048),...]
    all_to_all x2 -> x0, blocking collectives: 52.2 us -> none  [the longest x1 28.3 us: sent_collect(): lax.all_to_all(jnp.broadcast_to(value[None], (size, *value.shape)), axis,...]
    reduce_scatter x1 -> x0, waiting for transfers between devices: 27.9 us -> none  [on_device(): lax.psum_scatter(down_part.astype(jnp.bfloat16), 'tp', scatter_dimension=...]
    all_to_all x1 -> x0, waiting for transfers between devices: 17.5 us -> none  [on_device(): lax.all_to_all(summed, 'sp', split_axis=0, concat_axis=0, tiled=True)]
    dot_general x4 -> x0, matrix products: 17 us -> none  [the longest x1 8.22 us: on_device(): jnp.dot(hidden_act, expert_down[0], preferred_element_type=jnp.float32)]
    all_to_all x1 -> x0, starting transfers between devices: 10.9 us -> none  [on_device(): lax.all_to_all(summed, 'sp', split_axis=0, concat_axis=0, tiled=True)]
    reshape x4 -> x1, local copies, waits for them, and re-layouts: 6.07 us -> 1.32 us  [experts(): flat = routes.T.reshape(1, 64)]
    unnamed x27 -> x26, local copies, waits for them, and re-layouts: 8.53 us -> 12.7 us
  transfers between devices with their start and end apart: 2 -> 0, of which waited for: 2 -> 0; matrix products, arithmetic and copies ran while one was open for 0% -> 0% of each run, Pallas kernels for 0% -> 0%
where the time goes in v2:
time: 158 us; the launch traced here: 157 us
  Pallas kernels  141 us (89%)
  local copies, waits for them, and re-layouts  15.6 us (10%)
    pallas_call x1, Pallas kernels, experts(): pl.pallas_call(experts_kernel, out_shape=jax.ShapeDtypeStruct((32, 2048),...  73.7 us
    pallas_call x1, Pallas kernels, attend(): pl.pallas_call(attend_kernel, out_shape=(jax.ShapeDtypeStruct((32, 2048),...  67.2 us
    unnamed x26, local copies, waits for them, and re-layouts  12.7 us

profile of v2, /device:TPU:1, one launch (start us, length us, event | category | flops | bytes accessed | tf_op | source)
XLA Modules:
  0.0 157.3 jit_solution(2408611159179544148)
XLA Ops:
  0.0 1.3 reshape.51.rrow_hbm
  1.3 0.8 multiply_cosine_fusion
  2.1 0.1 cos.8
  2.2 0.1 sin.8
  2.3 1.4 copy.18.rw_hbm
  3.6 1.4 reshape_reshape.4.rcol_hbm
  5.0 0.0 copy-start
  5.0 1.6 %copy-done = bf16[512,2048]{1,0:T(8,128)(2,1)S(1)} copy-done((bf16[512,2048]{1,0:T(8,128)(2,1)S(1)}, bf16[512,2048]{1,0:T(8,128)(2,1)}, u32[]{:S(2)}) %copy-start) | copy-done | bytes 2097176
  6.6 0.9 copy-done.3
  7.5 0.0 copy-start.4
  7.5 0.9 copy-done.4
  8.4 0.8 copy-done.5
  9.2 0.8 copy-done.6
  10.0 0.8 copy-done.7
  10.7 0.8 copy-done.8
  11.5 0.7 copy-done.9
  12.2 0.7 copy-done.10
  12.8 0.7 copy-done.11
  13.5 67.2 %attend.1 = (f32[32,2048]{1,0:T(8,128)S(1)}, bf16[32,2048]{1,0:T(8,128)(2,1)S(1)}) custom-call(bf16[128,512]{1,0:T(8,128)(2,1)S(1)} %copy-done.3, bf16[128,128]{1,0:T(8,128)(2,1)S(1)} %copy-done.5, bf16[128,128]{1,0:T(8,128)(2,1)S(1)} %copy-done.6, f32[1,128]{1,0:T(1,128)S(1)} %bitcast.5, f32[1,128]{1,0:T(1,128)S(1)} %bitcast.6, ...), custom_call_target="tpu_custom_call" | custom-call | tf_op jit(solution)/shard_map/attend/pallas_call | solution.py:245
  80.7 0.0 copy-start.1
  80.7 0.7 copy-done.1
  81.4 0.7 copy-done.2
  82.1 73.7 %experts.1 = bf16[32,2048]{1,0:T(8,128)(2,1)} custom-call(bf16[32,2048]{1,0:T(8,128)(2,1)} %copy-done.2, f32[32,2048]{1,0:T(8,128)} %copy-done.1, s32[1,64]{1,0:T(1,128)} %reshape.51.rrow_hbm, s32[64,1]{1,0:T(8,128)} %reshape_reshape.4.rcol_hbm, f32[32,2]{1,0:T(8,128)} %copy.18.rw_hbm, bf16[1,2048,768]{2,1,0:T(8,128)(2,1)} %wg_hbm.1, ...), custom_call_target="tpu_custom_call" | custom-call | tf_op jit(solution)/shard_map/experts/pallas_call | solution.py:623
  155.8 1.6 copy.20
  (13 shorter events, 0.0 us)
Async XLA Ops:
  5.0 1.6 %copy-start = (bf16[512,2048]{1,0:T(8,128)(2,1)S(1)}, bf16[512,2048]{1,0:T(8,128)(2,1)}, u32[]{:S(2)}) copy-start(bf16[512,2048]{1,0:T(8,128)(2,1)} %outw_hbm.1) | copy-start | bytes 6291460
  6.6 0.9 copy-start.3
  7.5 0.9 copy-start.4
  8.4 0.8 copy-start.5
  9.2 0.8 copy-start.6
  10.0 0.8 copy-start.7
  10.7 0.8 copy-start.8
  11.5 0.7 copy-start.9
  12.2 0.7 copy-start.10
  12.8 0.7 copy-start.11
  80.7 0.7 copy-start.1
  81.4 0.7 copy-start.2
